TPU v7x, 32 devices: a whole 2x2x4 slice. The times are simulated.
32 devices in a mesh: dp: 4 (over y, x), kv: 4 (over z), tp: 2 (over core).
Axes of the slice: x: 2, y: 2, z: 4, core: 2. Of those that a mesh axis runs over, the one named last changes fastest.
Arguments:
- resid: bfloat16 [16, 2048], P('dp', ('kv', 'tp')), may hold values from -45 to 45
- norm_gain: bfloat16 [3, 2048], P(None, ('kv', 'tp')), may hold values from 0.099609375 to 1.8984375
- ffn_gate: bfloat16 [2, 2048, 5632], P(None, None, ('kv', 'tp')), may hold values from -0.125 to 0.125
- ffn_up: bfloat16 [2, 2048, 5632], P(None, None, ('kv', 'tp')), may hold values from -0.125 to 0.125
- ffn_down: bfloat16 [2, 5632, 2048], P(None, ('kv', 'tp')), may hold values from -0.109375 to 0.109375
- w_x: bfloat16 [2048, 64, 64], P(None, 'kv', 'tp'), may hold values from -0.125 to 0.125
- w_z: bfloat16 [2048, 64, 64], P(None, 'kv', 'tp'), may hold values from -0.125 to 0.125
- w_bc: bfloat16 [2048, 2, 8, 128], P('kv'), may hold values from -0.125 to 0.125
- w_dt: bfloat16 [2048, 64], P('kv'), may hold values from -0.125 to 0.125
- dt_bias: float32 [64], replicated, may hold values from -2 to 0.5
- a_log: float32 [64], replicated, may hold values from -1.5 to 1.5
- d_skip: float32 [64], replicated, may hold values from 0.5 to 1.5
- conv_wx: bfloat16 [4, 64, 64], P(None, None, 'tp'), may hold values from -3 to 3
- conv_wbc: bfloat16 [4, 2, 8, 128], replicated, may hold values from -3 to 3
- conv_x: bfloat16 [16, 3, 64, 64], P(('dp', 'kv'), None, None, 'tp'), may hold values from -6 to 6
- conv_bc: bfloat16 [16, 3, 2, 8, 128], P(('dp', 'kv')), may hold values from -6 to 6
- ssm_state: float32 [16, 64, 64, 128], P(('dp', 'kv'), None, 'tp'), may hold values from -3 to 3
- w_out: bfloat16 [64, 64, 2048], P(None, 'tp', 'kv'), may hold values from -0.09375 to 0.09375
Outputs:
- final: bfloat16 [16, 2048], P('dp', ('kv', 'tp'))
All inputs are finite; a program needn't handle non-finite values.
Results may differ from a plain program's by a relative error of at most 0.018.
Values may be sent and summed in bfloat16 or wider, within the bound.
No kernel may reach another device: no remote copies, remote signals or barrier semaphores. Data moves between devices by JAX's collectives and lax.ppermute only.
A program may use at most 64 MiB of HBM per device.

v0:
```python
import jax
import jax.numpy as jnp
from jax import lax
from jax.sharding import PartitionSpec as P

D = 2048
EPS = 1e-06


def normalize(rows, gain):
    values = rows.astype(jnp.float32)
    scale = lax.rsqrt(jnp.mean(values * values, axis=1, keepdims=True) + EPS)
    return (values * scale * gain.astype(jnp.float32).reshape(1, -1)).astype(jnp.bfloat16)


def feed_forward(normed, w_gate, w_up, w_down):
    gate = jnp.dot(normed, w_gate, preferred_element_type=jnp.float32)
    upper = jnp.dot(normed, w_up, preferred_element_type=jnp.float32)
    hidden = (jax.nn.silu(gate) * upper).astype(jnp.bfloat16)
    return jnp.dot(hidden, w_down, preferred_element_type=jnp.float32)


def add_half(base, sums):
    return (base.astype(jnp.float32) + 0.5 * sums).astype(jnp.bfloat16)


def ffn_totals(partial_value):
    return lax.psum(partial_value, ("kv", "tp"))


def short_conv(history, newest, taps):
    window = jnp.concatenate(
        [history.astype(jnp.float32), newest.astype(jnp.float32)[:, None]], axis=1
    )
    return jax.nn.silu(jnp.sum(window * taps.astype(jnp.float32)[None], axis=1))


def state_step(
    xs_new,
    zeta,
    bc_new,
    dt_raw,
    conv_x,
    conv_bc,
    ssm_state,
    conv_wx,
    conv_wbc,
    dt_bias,
    a_log,
    d_skip,
):
    xconv = short_conv(conv_x, xs_new, conv_wx)
    bconv = short_conv(conv_bc, bc_new, conv_wbc)
    heads = xconv.shape[1]
    groups = bconv.shape[2]
    bmat = jnp.repeat(bconv[:, 0], heads // groups, axis=1)
    cmat = jnp.repeat(bconv[:, 1], heads // groups, axis=1)
    step_size = jax.nn.softplus(dt_raw + dt_bias[None, :])
    decay = jnp.exp(-step_size * jnp.exp(a_log)[None, :])
    updated = (
        decay[:, :, None, None] * ssm_state
        + (step_size[:, :, None] * xconv)[..., None] * bmat[:, :, None, :]
    )
    mixed = (
        jnp.einsum("shpn,shn->shp", updated, cmat, precision=lax.Precision.HIGHEST)
        + d_skip[None, :, None] * xconv
    )
    return (mixed * jax.nn.silu(zeta.astype(jnp.float32))).astype(jnp.bfloat16)


def group_terms(slab, w_bc, w_dt):
    span = slab.shape[1]
    flat_bc = w_bc.reshape(span, -1)
    bc_part = jnp.dot(slab, flat_bc, preferred_element_type=jnp.float32)
    dt_part = jnp.dot(slab, w_dt, preferred_element_type=jnp.float32)
    return (
        lax.psum_scatter(bc_part, "kv", scatter_dimension=0, tiled=True),
        lax.psum_scatter(dt_part, "kv", scatter_dimension=0, tiled=True),
    )


def mix_partial(
    normed,
    w_x,
    w_z,
    w_bc,
    w_dt,
    dt_bias,
    a_log,
    d_skip,
    conv_wx,
    conv_wbc,
    conv_x,
    conv_bc,
    ssm_state,
    w_out,
):
    rows = normed.shape[0]
    local_heads = w_x.shape[1]
    half = w_x.shape[2]
    xs_part = (
        jnp.dot(normed, w_x.reshape(D, -1), preferred_element_type=jnp.float32)
        .astype(jnp.bfloat16)
        .reshape(rows, local_heads, half)
    )
    zeta_part = (
        jnp.dot(normed, w_z.reshape(D, -1), preferred_element_type=jnp.float32)
        .astype(jnp.bfloat16)
        .reshape(rows, local_heads, half)
    )
    xs_new, zeta = (
        lax.all_to_all(xs_part, "kv", split_axis=0, concat_axis=1, tiled=True),
        lax.all_to_all(zeta_part, "kv", split_axis=0, concat_axis=1, tiled=True),
    )
    span = w_bc.shape[0]
    slab = lax.dynamic_slice_in_dim(normed, lax.axis_index("kv") * span, span, 1)
    bc_sum, dt_raw = group_terms(slab, w_bc, w_dt)
    bc_new = bc_sum.astype(jnp.bfloat16).reshape((bc_sum.shape[0],) + w_bc.shape[1:])
    mixed = state_step(
        xs_new,
        zeta,
        bc_new,
        dt_raw,
        conv_x,
        conv_bc,
        ssm_state,
        conv_wx,
        conv_wbc,
        dt_bias,
        a_log,
        d_skip,
    )
    flat_out = w_out.reshape(-1, w_out.shape[2])
    piece = lax.all_gather(mixed, "kv", axis=0, tiled=True)
    return jnp.dot(piece.reshape(piece.shape[0], -1), flat_out, preferred_element_type=jnp.float32)


def per_device(
    resid,
    norm_gain,
    ffn_gate,
    ffn_up,
    ffn_down,
    w_x,
    w_z,
    w_bc,
    w_dt,
    dt_bias,
    a_log,
    d_skip,
    conv_wx,
    conv_wbc,
    conv_x,
    conv_bc,
    ssm_state,
    w_out,
):
    mixer_args = (
        w_x,
        w_z,
        w_bc,
        w_dt,
        dt_bias,
        a_log,
        d_skip,
        conv_wx,
        conv_wbc,
        conv_x,
        conv_bc,
        ssm_state,
        w_out,
    )
    rows, gains = (
        lax.all_gather(resid, ("kv", "tp"), axis=1, tiled=True),
        lax.all_gather(norm_gain, ("kv", "tp"), axis=1, tiled=True),
    )
    first = add_half(
        rows,
        ffn_totals(feed_forward(normalize(rows, gains[0]), ffn_gate[0], ffn_up[0], ffn_down[0])),
    )
    partial_value = mix_partial(normalize(first, gains[1]), *mixer_args)
    span = partial_value.shape[1]
    block = lax.dynamic_slice_in_dim(first, lax.axis_index("kv") * span, span, 1)
    joined = (block.astype(jnp.float32) + lax.psum(partial_value, "tp")).astype(jnp.bfloat16)
    second = lax.all_gather(joined, "kv", axis=1, tiled=True)
    final = add_half(
        second,
        ffn_totals(feed_forward(normalize(second, gains[2]), ffn_gate[1], ffn_up[1], ffn_down[1])),
    )
    width = resid.shape[1]
    return lax.dynamic_slice_in_dim(final, lax.axis_index(("kv", "tp")) * width, width, 1)


def solution(mesh):
    placed = (
        P("dp", ("kv", "tp")),
        P(None, ("kv", "tp")),
        P(None, None, ("kv", "tp")),
        P(None, None, ("kv", "tp")),
        P(None, ("kv", "tp"), None),
        P(None, "kv", "tp"),
        P(None, "kv", "tp"),
        P("kv", None, None, None),
        P("kv", None),
        P(),
        P(),
        P(),
        P(None, None, "tp"),
        P(),
        P(("dp", "kv"), None, None, "tp"),
        P(("dp", "kv"), None, None, None, None),
        P(("dp", "kv"), None, "tp", None),
        P(None, "tp", "kv"),
    )
    return jax.shard_map(
        per_device, mesh=mesh, in_specs=placed, out_specs=P("dp", ("kv", "tp")), check_vma=False
    )
```

profile of v0, /device:TPU:0, one launch (start us, length us, event | category | flops | bytes accessed | tf_op | source)
XLA Modules:
  0.0 168.5 jit_solution(16530086735748407296)
XLA Ops:
  0.0 14.7 %all_gather.12 = bf16[4,2048]{1,0:T(4,128)(2,1)S(1)} all-gather(bf16[4,256]{1,0:T(4,128)(2,1)} %param.18), channel_id=1, replica_groups=mesh['dp'=4,'kv'=4,'tp'=2] {'kv','tp'}, dimensions={1}, use_global_device_ids=true | all-gather | bytes 18432 | tf_op jit(solution)/shard_map/all_gather | solution.py:174
  14.9 12.9 %all_gather.13 = bf16[3,2048]{1,0:T(4,128)(2,1)S(1)} all-gather(bf16[3,256]{1,0:T(4,128)(2,1)} %param.19), channel_id=1, replica_groups=mesh['dp'=4,'kv'=4,'tp'=2] {'kv','tp'}, dimensions={1}, use_global_device_ids=true | all-gather | bytes 13824 | tf_op jit(solution)/shard_map/all_gather | solution.py:175
  27.8 2.7 %fusion.10 = f32[4,704]{1,0:T(4,128)S(1)} fusion(bf16[2,2048,704]{1,2,0:T(8,128)(2,1)} %param.20, bf16[4,2048]{1,0:T(4,128)(2,1)S(1)} %all_gather.12, f32[2048]{0:T(1024)S(1)} %bitcast.113, f32[4]{0:T(128)S(1)} %add_rsqrt_fusion.2), kind=kOutput, calls=%fused_computation.10 | convolution fusion | flops 11567104 | bytes 2919440 | tf_op jit(solution)/shard_map/dot_general | solution.py:17
  30.5 4.4 %fusion.6 = f32[4,2048]{1,0:T(4,128)S(1)} fusion(bf16[2,704,2048]{2,1,0:T(8,128)(2,1)} %param.22, bf16[2,2048,704]{1,2,0:T(8,128)(2,1)} %param.21, f32[4,704]{1,0:T(4,128)S(1)} %fusion.10, bf16[4,2048]{1,0:T(4,128)(2,1)S(1)} %all_gather.12, f32[2048]{0:T(1024)S(1)} %bitcast.114, f32[4]{0:T(128)S(1)} %add_rsqrt_fusion.2), kind=kOutput, calls=%fused_computation.6 | convolution fusion | flops 23118336 | bytes 5835792 | tf_op jit(solution)/shard_map/dot_general | solution.py:20
  34.8 26.7 %psum.21 = f32[4,2048]{1,0:T(4,128)S(1)} all-reduce(f32[4,2048]{1,0:T(4,128)S(1)} %fusion.6), channel_id=1, replica_groups=mesh['dp'=4,'kv'=4,'tp'=2] {'kv','tp'}, use_global_device_ids=true, to_apply=%region_1.2 | all-reduce | flops 8192 | bytes 65536 | tf_op jit(solution)/shard_map/psum | solution.py:28
  61.8 0.6 convolution_convert_fusion.1
  62.5 0.7 reshape.219
  63.2 3.2 %all-to-all-start = ((bf16[4,2,256]{2,1,0:T(2,128)(2,1)}), bf16[4,2,256]{2,1,0:T(2,128)(2,1)S(1)}, u32[]{:S(2)}, u32[]{:S(2)}) async-start(bf16[4,2,256]{2,1,0:T(2,128)(2,1)} %reshape.219), calls=%async_computation | async-start | bytes 8192 | tf_op jit(solution)/shard_map/all_to_all | solution.py:112
  66.5 2.2 %convolution_convert_fusion = bf16[4,512]{1,0:T(4,128)(2,1)S(1)} fusion(bf16[4,2048]{1,0:T(4,128)(2,1)S(1)} %fusion.47, bf16[2048,512]{0,1:T(8,128)(2,1)} %bitcast.109), kind=kOutput, calls=%fused_computation.26 | convolution fusion | flops 8390656 | bytes 2117632 | tf_op jit(solution)/shard_map/dot_general | solution.py:107
  68.9 2.0 %fusion.18 = f32[4,2048]{1,0:T(4,128)S(1)} fusion(bf16[64,8,16,128]{3,2,1,0:T(8,128)(2,1)} %bitcast.108, bf16[4,2048]{1,0:T(4,128)(2,1)S(1)} %fusion.47, s32[]{:T(128)S(6)} %select_n.11), kind=kOutput, calls=%fused_computation.18 | convolution fusion | flops 8388608 | bytes 2134020 | tf_op jit(solution)/shard_map/dot_general | solution.py:74
  71.4 19.8 %all-reduce.2 = (bf16[4,2048]{1,0:T(4,128)(2,1)S(1)}, f32[4,64]{1,0:T(4,128)S(1)}) all-reduce(f32[4,2048]{1,0:T(4,128)S(1)} %fusion.18, f32[4,64]{1,0:T(4,128)S(1)} %fusion.69), channel_id=4, replica_groups=mesh['dp'=4,'kv'=4,'tp'=2] {'kv'}, use_global_device_ids=true, to_apply=%region_5.6.clone | all-reduce | flops 8448 | bytes 51200
  91.2 0.7 fusion.60
  92.1 0.7 reshape.217
  92.8 3.2 %all-to-all-start.1 = ((bf16[4,2,256]{2,1,0:T(2,128)(2,1)}), bf16[4,2,256]{2,1,0:T(2,128)(2,1)S(1)}, u32[]{:S(2)}, u32[]{:S(2)}) async-start(bf16[4,2,256]{2,1,0:T(2,128)(2,1)} %reshape.217), calls=%async_computation.1 | async-start | bytes 8192 | tf_op jit(solution)/shard_map/all_to_all | solution.py:113
  96.0 0.7 fusion.75
  96.9 4.7 %all-to-all-done.1 = bf16[4,2,256]{2,1,0:T(2,128)(2,1)S(1)} async-done(((bf16[4,2,256]{2,1,0:T(2,128)(2,1)}), bf16[4,2,256]{2,1,0:T(2,128)(2,1)S(1)}, u32[]{:S(2)}, u32[]{:S(2)}) %all-to-all-start.1) | async-done | bytes 4128 | tf_op jit(solution)/shard_map/all_to_all | solution.py:113
  101.9 1.9 %fusion.33 = f32[64,1,32]{2,1,0:T(1,128)S(1)} fusion(f32[64,128,1]{1,2,0:T(1,128)S(1)} %bitcast.110, f32[1,64,32,128]{3,2,1,0:T(8,128)S(1)} %copy-done.1, f32[64,128]{1,0:T(8,128)S(1)} %broadcast_bitcast_fusion, f32[64,32]{1,0:T(8,128)S(1)} %copy.28, f32[64]{0:T(128)S(1)} %get-tuple-element.7), kind=kOutput, calls=%fused_computation.28 | convolution fusion | flops 3932160 | bytes 1130752 | tf_op jit(solution)/shard_map/shpn,shn->shp/dot_general | solution.py:65
  103.9 13.1 %all-gather.1 = bf16[4,64,32]{1,2,0:T(8,128)(2,1)S(1)} all-gather(bf16[1,64,32]{1,2,0:T(8,128)(2,1)S(1)} %fusion.64), channel_id=2, replica_groups=mesh['dp'=4,'kv'=4,'tp'=2] {'kv'}, dimensions={0}, use_global_device_ids=true | all-gather | bytes 20480 | tf_op jit(solution)/shard_map/all_gather | solution.py:134
  117.1 2.0 %convolution_bitcast_fusion = f32[4,512]{1,0:T(4,128)S(1)} fusion(bf16[4,64,32]{2,0,1:T(4,128)(2,1)S(1)} %copy.35, bf16[64,32,512]{2,1,0:T(8,128)(2,1)} %param.35), kind=kOutput, calls=%fused_computation.25 | convolution fusion | flops 8388608 | bytes 2121728 | tf_op jit(solution)/shard_map/dot_general | solution.py:135
  119.2 2.5 %psum.22 = f32[4,512]{1,0:T(4,128)S(1)} all-reduce(f32[4,512]{1,0:T(4,128)S(1)} %convolution_bitcast_fusion), channel_id=1, replica_groups=mesh['dp'=4,'kv'=4,'tp'=2] {'tp'}, use_global_device_ids=true, to_apply=%region_7.8 | all-reduce | flops 2048 | bytes 16384 | tf_op jit(solution)/shard_map/psum | solution.py:184
  121.6 13.2 %all_gather.15 = bf16[4,2048]{1,0:T(4,128)(2,1)S(1)} all-gather(bf16[4,512]{1,0:T(4,128)(2,1)S(1)} %add_convert_fusion), channel_id=1, replica_groups=mesh['dp'=4,'kv'=4,'tp'=2] {'kv'}, dimensions={1}, use_global_device_ids=true | all-gather | bytes 20480 | tf_op jit(solution)/shard_map/all_gather | solution.py:185
  135.0 2.7 %fusion.4 = f32[4,704]{1,0:T(4,128)S(1)} fusion(bf16[2,2048,704]{1,2,0:T(8,128)(2,1)} %param.20, f32[2048]{0:T(1024)S(1)} %bitcast.111, f32[4]{0:T(128)S(1)} %add_rsqrt_fusion, bf16[4,2048]{1,0:T(4,128)(2,1)S(1)} %all_gather.15), kind=kOutput, calls=%fused_computation.4 | convolution fusion | flops 11567104 | bytes 2919440 | tf_op jit(solution)/shard_map/dot_general | solution.py:17
  137.7 4.4 %fusion = f32[4,2048]{1,0:T(4,128)S(1)} fusion(bf16[2,704,2048]{2,1,0:T(8,128)(2,1)} %param.22, bf16[2,2048,704]{1,2,0:T(8,128)(2,1)} %param.21, f32[4,704]{1,0:T(4,128)S(1)} %fusion.4, f32[2048]{0:T(1024)S(1)} %bitcast.112, f32[4]{0:T(128)S(1)} %add_rsqrt_fusion, bf16[4,2048]{1,0:T(4,128)(2,1)S(1)} %all_gather.15), kind=kOutput, calls=%fused_computation | convolution fusion | flops 23118336 | bytes 5835792 | tf_op jit(solution)/shard_map/dot_general | solution.py:20
  142.0 25.9 %psum.23 = f32[4,2048]{1,0:T(4,128)S(1)} all-reduce(f32[4,2048]{1,0:T(4,128)S(1)} %fusion), channel_id=1, replica_groups=mesh['dp'=4,'kv'=4,'tp'=2] {'kv','tp'}, use_global_device_ids=true, to_apply=%region_9.10 | all-reduce | flops 8192 | bytes 65536 | tf_op jit(solution)/shard_map/psum | solution.py:28
  (54 shorter events, 2.8 us)
Async XLA Ops:
  0.0 61.7 %copy-start = (bf16[2048,16,32]{0,2,1:T(8,128)(2,1)S(1)}, bf16[2048,16,32]{0,2,1:T(8,128)(2,1)}, u32[]{:S(2)}) copy-start(bf16[2048,16,32]{0,2,1:T(8,128)(2,1)} %param.23) | copy-start | bytes 6291460
  34.8 33.9 %copy-start.2 = (bf16[512,64]{0,1:T(8,128)(2,1)S(1)}, bf16[512,64]{0,1:T(8,128)(2,1)}, u32[]{:S(2)}) copy-start(bf16[512,64]{0,1:T(8,128)(2,1)} %param.26) | copy-start | bytes 196612
  61.7 9.1 %copy-start.10 = (u32[32]{0:T(128)S(1)}, u32[32]{0:T(128)}, u32[]{:S(2)}) copy-start(u32[32]{0:T(128)} %constant.45) | copy-start | bytes 388
  61.7 30.2 %copy-start.5 = (bf16[4,2,8,128]{3,2,1,0:T(8,128)(2,1)S(1)}, bf16[4,2,8,128]{3,2,1,0:T(8,128)(2,1)}, u32[]{:S(2)}) copy-start(bf16[4,2,8,128]{3,2,1,0:T(8,128)(2,1)} %param.31) | copy-start | bytes 49156
  61.8 30.2 %copy-start.6 = (bf16[1,3,2,8,128]{4,3,2,1,0:T(8,128)(2,1)S(1)}, bf16[1,3,2,8,128]{4,3,2,1,0:T(8,128)(2,1)}, u32[]{:S(2)}) copy-start(bf16[1,3,2,8,128]{4,3,2,1,0:T(8,128)(2,1)} %param.33) | copy-start | bytes 36868
  61.8 34.2 %copy-start.8 = (f32[64]{0:T(128)S(1)}, f32[64]{0:T(128)}, u32[]{:S(2)}) copy-start(f32[64]{0:T(128)} %param.28) | copy-start | bytes 772
  61.8 34.2 %copy-start.9 = (f32[64]{0:T(128)S(1)}, f32[64]{0:T(128)}, u32[]{:S(2)}) copy-start(f32[64]{0:T(128)} %param.27) | copy-start | bytes 772
  62.4 39.3 %copy-start.3 = (bf16[4,64,32]{1,2,0:T(8,128)(2,1)S(1)}, bf16[4,64,32]{1,2,0:T(8,128)(2,1)}, u32[]{:S(2)}) copy-start(bf16[4,64,32]{1,2,0:T(8,128)(2,1)} %param.30) | copy-start | bytes 49156
  62.4 39.3 %copy-start.4 = (bf16[1,3,64,32]{2,3,1,0:T(8,128)(2,1)S(1)}, bf16[1,3,64,32]{2,3,1,0:T(8,128)(2,1)}, u32[]{:S(2)}) copy-start(bf16[1,3,64,32]{2,3,1,0:T(8,128)(2,1)} %param.32) | copy-start | bytes 36868
  62.4 39.4 %copy-start.1 = (f32[1,64,32,128]{3,2,1,0:T(8,128)S(1)}, f32[1,64,32,128]{3,2,1,0:T(8,128)}, u32[]{:S(2)}) copy-start(f32[1,64,32,128]{3,2,1,0:T(8,128)} %param.34) | copy-start | bytes 3145732
  63.2 29.5 %all-to-all-start = ((bf16[4,2,256]{2,1,0:T(2,128)(2,1)}), bf16[4,2,256]{2,1,0:T(2,128)(2,1)S(1)}, u32[]{:S(2)}, u32[]{:S(2)}) async-start(bf16[4,2,256]{2,1,0:T(2,128)(2,1)} %reshape.219), calls=%async_computation | async-start | bytes 8192 | tf_op jit(solution)/shard_map/all_to_all | solution.py:112
  66.5 37.4 %copy-start.7 = (f32[64]{0:T(128)S(1)}, f32[64]{0:T(128)}, u32[]{:S(2)}) copy-start(f32[64]{0:T(128)} %param.29) | copy-start | bytes 772
  92.8 8.8 %all-to-all-start.1 = ((bf16[4,2,256]{2,1,0:T(2,128)(2,1)}), bf16[4,2,256]{2,1,0:T(2,128)(2,1)S(1)}, u32[]{:S(2)}, u32[]{:S(2)}) async-start(bf16[4,2,256]{2,1,0:T(2,128)(2,1)} %reshape.217), calls=%async_computation.1 | async-start | bytes 8192 | tf_op jit(solution)/shard_map/all_to_all | solution.py:113
where the time goes:
time: 169 us
  blocking collectives  129 us (76%)
  matrix products  22.9 us (14%)
  starting transfers between devices  6.47 us (4%)
  waiting for transfers between devices  4.68 us (3%)
  local copies, waits for them, and re-layouts  3.47 us (2%)
  other arithmetic  1.89 us (1%)
    psum x2, blocking collectives, ffn_totals(): return lax.psum(partial_value, ('kv', 'tp'))  52.6 us
    unnamed x1, blocking collectives  19.8 us
    all_gather x1, blocking collectives, per_device(): lax.all_gather(resid, ('kv', 'tp'), axis=1, tiled=True)  14.7 us
    all_gather x1, blocking collectives, per_device(): second = lax.all_gather(joined, 'kv', axis=1, tiled=True)  13.2 us
    all_gather x1, blocking collectives, mix_partial(): piece = lax.all_gather(mixed, 'kv', axis=0, tiled=True)  13.1 us
    all_gather x1, blocking collectives, per_device(): lax.all_gather(norm_gain, ('kv', 'tp'), axis=1, tiled=True)  12.9 us
    dot_general x2, matrix products, feed_forward(): return jnp.dot(hidden, w_down, preferred_element_type=jnp.float32)  8.72 us
    dot_general x2, matrix products, feed_forward(): gate = jnp.dot(normed, w_gate, preferred_element_type=jnp.float32)  5.31 us
  transfers between devices with their start and end apart: 2, of which 1 were waited for; matrix products, arithmetic and copies ran while one was open for 4% of the time, Pallas kernels for 0%

commit v1 on v0

--- a/solution.py
+++ b/solution.py
@@ -25,7 +25,7 @@
 
 
 def ffn_totals(partial_value):
-    return lax.psum(partial_value, ("kv", "tp"))
+    return jnp.sum(lax.all_gather(partial_value, ("kv", "tp")), axis=0)
 
 
 def short_conv(history, newest, taps):

time: 169 us -> 144 us (0.85)
  blocking collectives: 129 us -> 105 us
    psum x2 -> x0, blocking collectives: 52.6 us -> none  [ffn_totals(): return lax.psum(partial_value, ('kv', 'tp'))]
    all_gather x0 -> x2, blocking collectives: none -> 28.5 us  [ffn_totals(): return jnp.sum(lax.all_gather(partial_value, ('kv', 'tp')), axis=0)]
  transfers between devices with their start and end apart: 2 -> 2, of which waited for: 1 -> 1; matrix products, arithmetic and copies ran while one was open for 4% -> 7% of each run, Pallas kernels for 0% -> 0%
where the time goes in v1:
time: 144 us; the launch traced here: 143 us
  blocking collectives  105 us (73%)
  matrix products  22.9 us (16%)
  starting transfers between devices  6.47 us (4%)
  local copies, waits for them, and re-layouts  3.49 us (2%)
  waiting for transfers between devices  3.27 us (2%)
  other arithmetic  1.99 us (1%)
    all_gather x2, blocking collectives, ffn_totals(): return jnp.sum(lax.all_gather(partial_value, ('kv', 'tp')), axis=0)  28.5 us
    unnamed x1, blocking collectives  19.8 us
    all_gather x1, blocking collectives, per_device(): lax.all_gather(resid, ('kv', 'tp'), axis=1, tiled=True)  14.7 us
    all_gather x1, blocking collectives, per_device(): second = lax.all_gather(joined, 'kv', axis=1, tiled=True)  13.2 us
    all_gather x1, blocking collectives, mix_partial(): piece = lax.all_gather(mixed, 'kv', axis=0, tiled=True)  13.1 us
    all_gather x1, blocking collectives, per_device(): lax.all_gather(norm_gain, ('kv', 'tp'), axis=1, tiled=True)  12.9 us
    dot_general x2, matrix products, feed_forward(): return jnp.dot(hidden, w_down, preferred_element_type=jnp.float32)  8.72 us
    dot_general x2, matrix products, feed_forward(): gate = jnp.dot(normed, w_gate, preferred_element_type=jnp.float32)  5.31 us
  transfers between devices with their start and end apart: 2, of which 1 were waited for; matrix products, arithmetic and copies ran while one was open for 7% of the time, Pallas kernels for 0%

profile of v1, /device:TPU:0, one launch (start us, length us, event | category | flops | bytes accessed | tf_op | source)
XLA Modules:
  0.0 143.1 jit_solution(3226332370910253282)
XLA Ops:
  0.0 14.7 %all_gather.24 = bf16[4,2048]{1,0:T(4,128)(2,1)S(1)} all-gather(bf16[4,256]{1,0:T(4,128)(2,1)} %param.18), channel_id=1, replica_groups=mesh['dp'=4,'kv'=4,'tp'=2] {'kv','tp'}, dimensions={1}, use_global_device_ids=true | all-gather | bytes 18432 | tf_op jit(solution)/shard_map/all_gather | solution.py:174
  14.9 12.9 %all_gather.25 = bf16[3,2048]{1,0:T(4,128)(2,1)S(1)} all-gather(bf16[3,256]{1,0:T(4,128)(2,1)} %param.19), channel_id=1, replica_groups=mesh['dp'=4,'kv'=4,'tp'=2] {'kv','tp'}, dimensions={1}, use_global_device_ids=true | all-gather | bytes 13824 | tf_op jit(solution)/shard_map/all_gather | solution.py:175
  27.8 2.7 %fusion.10 = f32[4,704]{1,0:T(4,128)S(1)} fusion(bf16[2,2048,704]{1,2,0:T(8,128)(2,1)} %param.20, bf16[4,2048]{1,0:T(4,128)(2,1)S(1)} %all_gather.24, f32[2048]{0:T(1024)S(1)} %bitcast.121, f32[4]{0:T(128)S(1)} %add_rsqrt_fusion.2), kind=kOutput, calls=%fused_computation.10 | convolution fusion | flops 11567104 | bytes 2919440 | tf_op jit(solution)/shard_map/dot_general | solution.py:17
  30.5 4.4 %fusion.18 = f32[1,4,2048]{2,1,0:T(4,128)S(1)} fusion(bf16[2,704,2048]{2,1,0:T(8,128)(2,1)} %param.22, bf16[2,2048,704]{1,2,0:T(8,128)(2,1)} %param.21, f32[4,704]{1,0:T(4,128)S(1)} %fusion.10, bf16[4,2048]{1,0:T(4,128)(2,1)S(1)} %all_gather.24, f32[2048]{0:T(1024)S(1)} %bitcast.122, f32[4]{0:T(128)S(1)} %add_rsqrt_fusion.2), kind=kOutput, calls=%fused_computation.18 | convolution fusion | flops 23118336 | bytes 5835792 | tf_op jit(solution)/shard_map/dot_general | solution.py:20
  34.8 14.3 %all-gather.3 = f32[8,4,2048]{2,1,0:T(4,128)S(1)} all-gather(f32[1,4,2048]{2,1,0:T(4,128)S(1)} %fusion.18), channel_id=2, replica_groups=mesh['dp'=4,'kv'=4,'tp'=2] {'kv','tp'}, dimensions={0}, use_global_device_ids=true | all-gather | bytes 294912 | tf_op jit(solution)/shard_map/all_gather | solution.py:28
  49.5 0.6 convolution_convert_fusion.1
  50.2 0.7 reshape.227
  50.9 3.2 %all-to-all-start = ((bf16[4,2,256]{2,1,0:T(2,128)(2,1)}), bf16[4,2,256]{2,1,0:T(2,128)(2,1)S(1)}, u32[]{:S(2)}, u32[]{:S(2)}) async-start(bf16[4,2,256]{2,1,0:T(2,128)(2,1)} %reshape.227), calls=%async_computation | async-start | bytes 8192 | tf_op jit(solution)/shard_map/all_to_all | solution.py:112
  54.2 2.0 %fusion.24 = f32[4,2048]{1,0:T(4,128)S(1)} fusion(bf16[64,8,16,128]{3,2,1,0:T(8,128)(2,1)} %bitcast.116, bf16[4,2048]{1,0:T(4,128)(2,1)S(1)} %fusion.53, s32[]{:T(128)S(6)} %select_n.11), kind=kOutput, calls=%fused_computation.20 | convolution fusion | flops 8388608 | bytes 2134020 | tf_op jit(solution)/shard_map/dot_general | solution.py:74
  56.3 19.8 %all-reduce.2 = (bf16[4,2048]{1,0:T(4,128)(2,1)S(1)}, f32[4,64]{1,0:T(4,128)S(1)}) all-reduce(f32[4,2048]{1,0:T(4,128)S(1)} %fusion.24, f32[4,64]{1,0:T(4,128)S(1)} %fusion.75), channel_id=6, replica_groups=mesh['dp'=4,'kv'=4,'tp'=2] {'kv'}, use_global_device_ids=true, to_apply=%region_5.6.clone | all-reduce | flops 8448 | bytes 51200
  76.7 0.7 fusion.66
  77.4 2.2 %convolution_convert_fusion = bf16[4,512]{1,0:T(4,128)(2,1)S(1)} fusion(bf16[4,2048]{1,0:T(4,128)(2,1)S(1)} %fusion.53, bf16[2048,512]{0,1:T(8,128)(2,1)} %bitcast.117), kind=kOutput, calls=%fused_computation.28 | convolution fusion | flops 8390656 | bytes 2117632 | tf_op jit(solution)/shard_map/dot_general | solution.py:107
  79.7 0.7 fusion.81
  80.5 0.7 reshape.225
  81.2 3.2 %all-to-all-start.1 = ((bf16[4,2,256]{2,1,0:T(2,128)(2,1)}), bf16[4,2,256]{2,1,0:T(2,128)(2,1)S(1)}, u32[]{:S(2)}, u32[]{:S(2)}) async-start(bf16[4,2,256]{2,1,0:T(2,128)(2,1)} %reshape.225), calls=%async_computation.1 | async-start | bytes 8192 | tf_op jit(solution)/shard_map/all_to_all | solution.py:113
  84.7 1.9 %fusion.39 = f32[64,1,32]{2,1,0:T(1,128)S(1)} fusion(f32[64,128,1]{1,2,0:T(1,128)S(1)} %bitcast.118, f32[1,64,32,128]{3,2,1,0:T(8,128)S(1)} %copy-done.1, f32[64,128]{1,0:T(8,128)S(1)} %broadcast_bitcast_fusion, f32[64,32]{1,0:T(8,128)S(1)} %copy.28, f32[64]{0:T(128)S(1)} %get-tuple-element.7), kind=kOutput, calls=%fused_computation.30 | convolution fusion | flops 3932160 | bytes 1130752 | tf_op jit(solution)/shard_map/shpn,shn->shp/dot_general | solution.py:65
  86.7 3.3 %all-to-all-done.1 = bf16[4,2,256]{2,1,0:T(2,128)(2,1)S(1)} async-done(((bf16[4,2,256]{2,1,0:T(2,128)(2,1)}), bf16[4,2,256]{2,1,0:T(2,128)(2,1)S(1)}, u32[]{:S(2)}, u32[]{:S(2)}) %all-to-all-start.1) | async-done | bytes 4128 | tf_op jit(solution)/shard_map/all_to_all | solution.py:113
  90.2 13.1 %all-gather.4 = bf16[4,64,32]{1,2,0:T(8,128)(2,1)S(1)} all-gather(bf16[1,64,32]{1,2,0:T(8,128)(2,1)S(1)} %fusion.70), channel_id=3, replica_groups=mesh['dp'=4,'kv'=4,'tp'=2] {'kv'}, dimensions={0}, use_global_device_ids=true | all-gather | bytes 20480 | tf_op jit(solution)/shard_map/all_gather | solution.py:134
  103.4 2.0 %convolution_bitcast_fusion = f32[4,512]{1,0:T(4,128)S(1)} fusion(bf16[4,64,32]{2,0,1:T(4,128)(2,1)S(1)} %copy.35, bf16[64,32,512]{2,1,0:T(8,128)(2,1)} %param.35), kind=kOutput, calls=%fused_computation.27 | convolution fusion | flops 8388608 | bytes 2121728 | tf_op jit(solution)/shard_map/dot_general | solution.py:135
  105.5 2.5 %psum.7 = f32[4,512]{1,0:T(4,128)S(1)} all-reduce(f32[4,512]{1,0:T(4,128)S(1)} %convolution_bitcast_fusion), channel_id=1, replica_groups=mesh['dp'=4,'kv'=4,'tp'=2] {'tp'}, use_global_device_ids=true, to_apply=%region_7.8 | all-reduce | flops 2048 | bytes 16384 | tf_op jit(solution)/shard_map/psum | solution.py:184
  107.9 13.2 %all_gather.29 = bf16[4,2048]{1,0:T(4,128)(2,1)S(1)} all-gather(bf16[4,512]{1,0:T(4,128)(2,1)S(1)} %add_convert_fusion), channel_id=1, replica_groups=mesh['dp'=4,'kv'=4,'tp'=2] {'kv'}, dimensions={1}, use_global_device_ids=true | all-gather | bytes 20480 | tf_op jit(solution)/shard_map/all_gather | solution.py:185
  121.3 2.7 %fusion.4 = f32[4,704]{1,0:T(4,128)S(1)} fusion(bf16[2,2048,704]{1,2,0:T(8,128)(2,1)} %param.20, f32[2048]{0:T(1024)S(1)} %bitcast.119, f32[4]{0:T(128)S(1)} %add_rsqrt_fusion, bf16[4,2048]{1,0:T(4,128)(2,1)S(1)} %all_gather.29), kind=kOutput, calls=%fused_computation.4 | convolution fusion | flops 11567104 | bytes 2919440 | tf_op jit(solution)/shard_map/dot_general | solution.py:17
  124.0 4.4 %fusion.21 = f32[1,4,2048]{2,1,0:T(4,128)S(1)} fusion(bf16[2,704,2048]{2,1,0:T(8,128)(2,1)} %param.22, bf16[2,2048,704]{1,2,0:T(8,128)(2,1)} %param.21, f32[4,704]{1,0:T(4,128)S(1)} %fusion.4, f32[2048]{0:T(1024)S(1)} %bitcast.120, f32[4]{0:T(128)S(1)} %add_rsqrt_fusion, bf16[4,2048]{1,0:T(4,128)(2,1)S(1)} %all_gather.29), kind=kOutput, calls=%fused_computation.19 | convolution fusion | flops 23118336 | bytes 5835792 | tf_op jit(solution)/shard_map/dot_general | solution.py:20
  128.3 14.2 %all-gather.5 = f32[8,4,2048]{2,1,0:T(4,128)S(1)} all-gather(f32[1,4,2048]{2,1,0:T(4,128)S(1)} %fusion.21), channel_id=4, replica_groups=mesh['dp'=4,'kv'=4,'tp'=2] {'kv','tp'}, dimensions={0}, use_global_device_ids=true | all-gather | bytes 294912 | tf_op jit(solution)/shard_map/all_gather | solution.py:28
  (56 shorter events, 2.9 us)
Async XLA Ops:
  0.0 49.4 %copy-start = (bf16[2048,16,32]{0,2,1:T(8,128)(2,1)S(1)}, bf16[2048,16,32]{0,2,1:T(8,128)(2,1)}, u32[]{:S(2)}) copy-start(bf16[2048,16,32]{0,2,1:T(8,128)(2,1)} %param.23) | copy-start | bytes 6291460
  34.8 21.4 %copy-start.2 = (bf16[512,64]{0,1:T(8,128)(2,1)S(1)}, bf16[512,64]{0,1:T(8,128)(2,1)}, u32[]{:S(2)}) copy-start(bf16[512,64]{0,1:T(8,128)(2,1)} %param.26) | copy-start | bytes 196612
  34.8 41.3 %copy-start.10 = (u32[32]{0:T(128)S(1)}, u32[32]{0:T(128)}, u32[]{:S(2)}) copy-start(u32[32]{0:T(128)} %constant.45) | copy-start | bytes 388
  34.8 42.5 %copy-start.5 = (bf16[4,2,8,128]{3,2,1,0:T(8,128)(2,1)S(1)}, bf16[4,2,8,128]{3,2,1,0:T(8,128)(2,1)}, u32[]{:S(2)}) copy-start(bf16[4,2,8,128]{3,2,1,0:T(8,128)(2,1)} %param.31) | copy-start | bytes 49156
  34.8 42.6 %copy-start.6 = (bf16[1,3,2,8,128]{4,3,2,1,0:T(8,128)(2,1)S(1)}, bf16[1,3,2,8,128]{4,3,2,1,0:T(8,128)(2,1)}, u32[]{:S(2)}) copy-start(bf16[1,3,2,8,128]{4,3,2,1,0:T(8,128)(2,1)} %param.33) | copy-start | bytes 36868
  49.5 30.2 %copy-start.8 = (f32[64]{0:T(128)S(1)}, f32[64]{0:T(128)}, u32[]{:S(2)}) copy-start(f32[64]{0:T(128)} %param.28) | copy-start | bytes 772
  49.5 30.2 %copy-start.9 = (f32[64]{0:T(128)S(1)}, f32[64]{0:T(128)}, u32[]{:S(2)}) copy-start(f32[64]{0:T(128)} %param.27) | copy-start | bytes 772
  49.5 35.1 %copy-start.3 = (bf16[4,64,32]{1,2,0:T(8,128)(2,1)S(1)}, bf16[4,64,32]{1,2,0:T(8,128)(2,1)}, u32[]{:S(2)}) copy-start(bf16[4,64,32]{1,2,0:T(8,128)(2,1)} %param.30) | copy-start | bytes 49156
  49.5 35.1 %copy-start.4 = (bf16[1,3,64,32]{2,3,1,0:T(8,128)(2,1)S(1)}, bf16[1,3,64,32]{2,3,1,0:T(8,128)(2,1)}, u32[]{:S(2)}) copy-start(bf16[1,3,64,32]{2,3,1,0:T(8,128)(2,1)} %param.32) | copy-start | bytes 36868
  50.1 34.6 %copy-start.1 = (f32[1,64,32,128]{3,2,1,0:T(8,128)S(1)}, f32[1,64,32,128]{3,2,1,0:T(8,128)}, u32[]{:S(2)}) copy-start(f32[1,64,32,128]{3,2,1,0:T(8,128)} %param.34) | copy-start | bytes 3145732
  50.9 30.2 %all-to-all-start = ((bf16[4,2,256]{2,1,0:T(2,128)(2,1)}), bf16[4,2,256]{2,1,0:T(2,128)(2,1)S(1)}, u32[]{:S(2)}, u32[]{:S(2)}) async-start(bf16[4,2,256]{2,1,0:T(2,128)(2,1)} %reshape.227), calls=%async_computation | async-start | bytes 8192 | tf_op jit(solution)/shard_map/all_to_all | solution.py:112
  54.2 36.0 %copy-start.7 = (f32[64]{0:T(128)S(1)}, f32[64]{0:T(128)}, u32[]{:S(2)}) copy-start(f32[64]{0:T(128)} %param.29) | copy-start | bytes 772
  81.2 8.8 %all-to-all-start.1 = ((bf16[4,2,256]{2,1,0:T(2,128)(2,1)}), bf16[4,2,256]{2,1,0:T(2,128)(2,1)S(1)}, u32[]{:S(2)}, u32[]{:S(2)}) async-start(bf16[4,2,256]{2,1,0:T(2,128)(2,1)} %reshape.225), calls=%async_computation.1 | async-start | bytes 8192 | tf_op jit(solution)/shard_map/all_to_all | solution.py:113
